TPU v7x, 32 devices: a whole 2x2x4 slice. The times are simulated.
32 devices in a mesh: grp: 2 (over y), fs: 4 (over z), tp: 4 (over x, core).
Axes of the slice: x: 2, y: 2, z: 4, core: 2. Of those that a mesh axis runs over, the one named last changes fastest.
Arguments:
- tokens: bfloat16 [2048, 2048], P(('grp', 'fs')), parts along dimension 0, may hold values from -6 to 6
- ffn_pre_gain: bfloat16 [2048], replicated, may hold values from 0.099609375 to 1.8984375
- gate_weight: bfloat16 [2048, 5632], P('fs', 'tp'), may hold values from -0.125 to 0.125
- up_weight: bfloat16 [2048, 5632], P('fs', 'tp'), may hold values from -0.125 to 0.125
- down_weight: bfloat16 [5632, 2048], P('tp', 'fs'), may hold values from -0.078125 to 0.078125
- ffn_post_gain: bfloat16 [2048], replicated, may hold values from 0.099609375 to 1.8984375
- mix_pre_gain: bfloat16 [2048], replicated, may hold values from 0.099609375 to 1.8984375
- mix_u_weight: bfloat16 [2048, 2048], P('fs', 'tp'), may hold values from -0.125 to 0.125
- mix_v_weight: bfloat16 [2048, 2048], P('fs', 'tp'), may hold values from -0.125 to 0.125
- spatial_gain: bfloat16 [2048], P('tp'), may hold values from 0.099609375 to 1.8984375
- spatial_weight: bfloat16 [16, 128, 128], P('tp'), may hold values from -0.5 to 0.5
- spatial_bias: bfloat16 [16, 128], P('tp'), may hold values from 0.099609375 to 1.8984375
- mix_out_weight: bfloat16 [2048, 2048], P('tp', 'fs'), may hold values from -0.125 to 0.125
- mix_post_gain: bfloat16 [2048], replicated, may hold values from 0.099609375 to 1.8984375
- late_pre_gain: bfloat16 [2048], replicated, may hold values from 0.099609375 to 1.8984375
- late_post_gain: bfloat16 [2048], replicated, may hold values from 0.099609375 to 1.8984375
Outputs:
- result: bfloat16 [2048, 2048], P(('grp', 'fs')), parts along dimension 0
There are 2 independent parts, one for each index of `grp`. A program takes and returns all parts, laid end to end along the dimension named above; an argument that names none is the same for every part. Nothing has to cross between parts.
All inputs are finite; a program needn't handle non-finite values.
Results may differ from a plain program's by a relative error of at most 0.019.
Values may be sent and summed in bfloat16 or wider, within the bound.
No kernel may reach another device: no remote copies, remote signals or barrier semaphores. Data moves between devices by JAX's collectives and lax.ppermute only.
A program may use at most 128 MiB of HBM per device.

v0:
```python
import jax
import jax.numpy as jnp
from jax import lax
from jax.sharding import PartitionSpec as P

GROUP_WIDTH = 128
BLOCK = 128


def row_norm(values, gain):
    scale = lax.rsqrt(jnp.mean(values * values, axis=-1, keepdims=True) + 1e-06)
    return values * scale * gain.astype(jnp.float32)


def reduce_partial(terms):
    return lax.psum(terms.astype(jnp.bfloat16), "tp").astype(jnp.float32)


def add_branch(stream, terms, gain, factor):
    total = reduce_partial(terms)
    return (stream.astype(jnp.float32) + factor * row_norm(total, gain)).astype(jnp.bfloat16)


def gated_hidden(normed, gate_full, up_full):
    gate = jnp.dot(normed, gate_full, preferred_element_type=jnp.float32)
    upper = jnp.dot(normed, up_full, preferred_element_type=jnp.float32)
    return (jax.nn.silu(gate) * upper).astype(jnp.bfloat16)


def spatial_mix(u_linear, v_linear, spatial_gain, spatial_weight, spatial_bias):
    count = u_linear.shape[0]
    gated_u = jax.nn.gelu(u_linear, approximate=False)
    gating_v = jax.nn.gelu(v_linear, approximate=False)
    groups = gating_v.shape[1] // GROUP_WIDTH
    grouped = gating_v.reshape(count, groups, GROUP_WIDTH)
    centred = grouped - jnp.mean(grouped, axis=-1, keepdims=True)
    vnorm = centred * lax.rsqrt(jnp.mean(centred * centred, axis=-1, keepdims=True) + 1e-05)
    vnorm = (vnorm * spatial_gain.astype(jnp.float32).reshape(groups, GROUP_WIDTH)).astype(
        jnp.bfloat16
    )
    blocks = vnorm.reshape(count // BLOCK, BLOCK, groups, GROUP_WIDTH)
    lower = jnp.tril(jnp.ones((BLOCK, BLOCK), dtype=bool))
    masked = jnp.where(lower[None], spatial_weight, jnp.zeros_like(spatial_weight))
    spatial = jnp.einsum("gts,nsgc->ntgc", masked, blocks, preferred_element_type=jnp.float32)
    spatial = spatial + spatial_bias.astype(jnp.float32).T[None, :, :, None]
    return (gated_u * spatial.reshape(count, groups * GROUP_WIDTH)).astype(jnp.bfloat16)


def shards(
    tokens,
    ffn_pre_gain,
    gate_weight,
    up_weight,
    down_weight,
    ffn_post_gain,
    mix_pre_gain,
    mix_u_weight,
    mix_v_weight,
    spatial_gain,
    spatial_weight,
    spatial_bias,
    mix_out_weight,
    mix_post_gain,
    late_pre_gain,
    late_post_gain,
):
    normed = row_norm(tokens.astype(jnp.float32), ffn_pre_gain).astype(jnp.bfloat16)
    gate_full, up_full = (
        lax.all_gather(gate_weight, "fs", axis=0, tiled=True),
        lax.all_gather(up_weight, "fs", axis=0, tiled=True),
    )
    down_full = lax.all_gather(down_weight, "fs", axis=1, tiled=True)
    hidden = gated_hidden(normed, gate_full, up_full)
    terms = jnp.dot(hidden, down_full, preferred_element_type=jnp.float32)
    first = add_branch(tokens, terms, ffn_post_gain, 0.5)
    normed = row_norm(first.astype(jnp.float32), mix_pre_gain).astype(jnp.bfloat16)
    u_full, v_full = (
        lax.all_gather(mix_u_weight, "fs", axis=0, tiled=True),
        lax.all_gather(mix_v_weight, "fs", axis=0, tiled=True),
    )
    u_linear = jnp.dot(normed, u_full, preferred_element_type=jnp.float32)
    v_linear = jnp.dot(normed, v_full, preferred_element_type=jnp.float32)
    mixed = spatial_mix(u_linear, v_linear, spatial_gain, spatial_weight, spatial_bias)
    out_full = lax.all_gather(mix_out_weight, "fs", axis=1, tiled=True)
    terms = jnp.dot(mixed, out_full, preferred_element_type=jnp.float32)
    second = add_branch(first, terms, mix_post_gain, 1.0)
    normed = row_norm(second.astype(jnp.float32), late_pre_gain).astype(jnp.bfloat16)
    hidden = gated_hidden(normed, gate_full, up_full)
    terms = jnp.dot(hidden, down_full, preferred_element_type=jnp.float32)
    return add_branch(second, terms, late_post_gain, 0.5)


def solution(mesh):
    in_specs = (
        P(("grp", "fs"), None),
        P(),
        P("fs", "tp"),
        P("fs", "tp"),
        P("tp", "fs"),
        P(),
        P(),
        P("fs", "tp"),
        P("fs", "tp"),
        P("tp"),
        P("tp", None, None),
        P("tp", None),
        P("tp", "fs"),
        P(),
        P(),
        P(),
    )
    out_specs = P(("grp", "fs"), None)
    return jax.shard_map(shards, mesh=mesh, in_specs=in_specs, out_specs=out_specs, check_vma=False)
```

profile of v0, /device:TPU:0, one launch (start us, length us, event | category | flops | bytes accessed | tf_op | source)
XLA Modules:
  0.0 620.2 jit_solution(5151979985591970159)
XLA Ops:
  6.5 0.7 all-gather.7.cloned.1.call-update
  7.3 0.7 all-gather.11.cloned.1.call-update
  9.1 109.2 %all-gather.7.cloned.1.call-done = bf16[2048,1408]{1,0:T(8,128)(2,1)} async-done(((bf16[512,1408]{1,0:T(8,128)(2,1)}), bf16[2048,1408]{1,0:T(8,128)(2,1)}) %all-gather.7.cloned.1.call-update) | async-done | bytes 5767184 | tf_op jit(solution)/shard_map/all_gather | solution.py:69
  118.3 4.5 fusion.59
  122.8 102.0 %all-gather.11.cloned.1.call-done = bf16[1408,2048]{1,0:T(8,128)(2,1)} async-done(((bf16[1408,512]{1,0:T(8,128)(2,1)}), bf16[1408,2048]{1,0:T(8,128)(2,1)}) %all-gather.11.cloned.1.call-update) | async-done | bytes 5767184 | tf_op jit(solution)/shard_map/all_gather | solution.py:72
  224.9 106.6 %all-gather.9.cloned.1.call-done = bf16[2048,1408]{1,0:T(8,128)(2,1)} async-done(((bf16[512,1408]{1,0:T(8,128)(2,1)}), bf16[2048,1408]{1,0:T(8,128)(2,1)}) %all-gather.9.cloned.1.call-update) | async-done | bytes 5767184 | tf_op jit(solution)/shard_map/all_gather | solution.py:70
  331.4 8.9 %convolution_convert_fusion.2 = bf16[256,2048]{1,0:T(8,128)(2,1)} fusion(bf16[1408,2048]{1,0:T(8,128)(2,1)} %all-gather.11.cloned.1.call-done, bf16[2048,1408]{1,0:T(8,128)(2,1)} %all-gather.9.cloned.1.call-done, f32[256,1408]{1,0:T(8,128)S(1)} %fusion.59, bf16[256,2048]{1,0:T(8,128)(2,1)S(1)} %copy-done, f32[2048]{0:T(1024)S(1)} %convert_element_type.82, ...), kind=kOutput, calls=%fused_computation.21 | convolution fusion | flops 2957574144 | bytes 15082496 | tf_op jit(solution)/shard_map/dot_general | solution.py:74
  341.6 0.7 all-gather.17.cloned.1.call-update
  342.7 32.4 %all-reduce.4.cloned.1.call-done = bf16[256,2048]{1,0:T(8,128)(2,1)} async-done(((bf16[256,2048]{1,0:T(8,128)(2,1)}), bf16[256,2048]{1,0:T(8,128)(2,1)}) %all-reduce.4.cloned.1.call-update) | async-done | bytes 1048592 | tf_op jit(solution)/shard_map/psum | solution.py:16
  375.1 1.5 fusion.2
  376.6 2.0 fusion.14
  378.6 44.1 %all-gather.15.cloned.1.call-done = bf16[2048,512]{1,0:T(8,128)(2,1)} async-done(((bf16[512,512]{1,0:T(8,128)(2,1)}), bf16[2048,512]{1,0:T(8,128)(2,1)}) %all-gather.15.cloned.1.call-update) | async-done | bytes 2097168 | tf_op jit(solution)/shard_map/all_gather | solution.py:79
  422.7 3.4 fusion.28
  428.5 40.1 %all-gather.13.cloned.1.call-done = bf16[2048,512]{1,0:T(8,128)(2,1)} async-done(((bf16[512,512]{1,0:T(8,128)(2,1)}), bf16[2048,512]{1,0:T(8,128)(2,1)}) %all-gather.13.cloned.1.call-update) | async-done | bytes 2097168 | tf_op jit(solution)/shard_map/all_gather | solution.py:78
  468.6 46.1 %all-gather.17.cloned.1.call-done = bf16[512,2048]{1,0:T(8,128)(2,1)} async-done(((bf16[512,512]{1,0:T(8,128)(2,1)}), bf16[512,2048]{1,0:T(8,128)(2,1)}) %all-gather.17.cloned.1.call-update) | async-done | bytes 2097168 | tf_op jit(solution)/shard_map/all_gather | solution.py:84
  514.7 5.7 convolution_convert_fusion
  520.7 34.9 %all-reduce.6.cloned.1.call-done = bf16[256,2048]{1,0:T(8,128)(2,1)} async-done(((bf16[256,2048]{1,0:T(8,128)(2,1)}), bf16[256,2048]{1,0:T(8,128)(2,1)}) %all-reduce.6.cloned.1.call-update) | async-done | bytes 1048592 | tf_op jit(solution)/shard_map/psum | solution.py:16
  555.7 1.5 fusion.5
  557.2 1.9 fusion.18
  559.1 4.5 fusion.45
  563.6 8.9 %convolution_convert_fusion.1 = bf16[256,2048]{1,0:T(8,128)(2,1)} fusion(bf16[1408,2048]{1,0:T(8,128)(2,1)} %all-gather.11.cloned.1.call-done, bf16[2048,1408]{1,0:T(8,128)(2,1)} %all-gather.9.cloned.1.call-done, f32[256,1408]{1,0:T(8,128)S(1)} %fusion.45, bf16[256,2048]{1,0:T(8,128)(2,1)S(1)} %get-tuple-element.6, f32[2048]{0:T(1024)S(1)} %convert_element_type.99, ...), kind=kOutput, calls=%fused_computation.20 | convolution fusion | flops 2957574144 | bytes 15082496 | tf_op jit(solution)/shard_map/dot_general | solution.py:89
  572.5 36.9 %all-reduce.8.cloned.1.call-done = bf16[256,2048]{1,0:T(8,128)(2,1)} async-done(((bf16[256,2048]{1,0:T(8,128)(2,1)}), bf16[256,2048]{1,0:T(8,128)(2,1)}) %all-reduce.8.cloned.1.call-update) | async-done | bytes 1048592 | tf_op jit(solution)/shard_map/psum | solution.py:16
  609.4 1.5 fusion.7
  610.9 2.8 fusion.21
  (62 shorter events, 5.2 us)
Async XLA Ops:
  6.5 2.3 copy-start.2
  6.5 2.3 copy-start
  6.5 111.8 %all-gather.7.cloned.1.call-start = ((), (), s32[]{:S(2)}) async-start(), calls=%async_computation | async-start | bytes 7208960 | tf_op jit(solution)/shard_map/all_gather | solution.py:69
  7.3 217.6 %all-gather.11.cloned.1.call-start = ((), (), s32[]{:S(2)}) async-start(), calls=%async_computation.2 | async-start | bytes 7208960 | tf_op jit(solution)/shard_map/all_gather | solution.py:72
  8.0 323.4 %all-gather.9.cloned.1.call-start = ((), (), s32[]{:S(2)}) async-start(), calls=%async_computation.1 | async-start | bytes 7208960 | tf_op jit(solution)/shard_map/all_gather | solution.py:70
  8.7 366.4 %all-reduce.4.cloned.1.call-start = ((), (), s32[]{:S(2)}) async-start(), calls=%async_computation.3 | async-start | bytes 2097152 | tf_op jit(solution)/shard_map/psum | solution.py:16
  340.4 2.2 copy-start.3
  340.4 2.2 copy-start.4
  340.4 2.2 copy-start.8
  340.4 2.3 copy-start.9
  340.4 82.3 %all-gather.15.cloned.1.call-start = ((), (), s32[]{:S(2)}) async-start(), calls=%async_computation.5 | async-start | bytes 2621440 | tf_op jit(solution)/shard_map/all_gather | solution.py:79
  341.0 127.6 %all-gather.13.cloned.1.call-start = ((), (), s32[]{:S(2)}) async-start(), calls=%async_computation.4 | async-start | bytes 2621440 | tf_op jit(solution)/shard_map/all_gather | solution.py:78
  341.6 173.1 %all-gather.17.cloned.1.call-start = ((), (), s32[]{:S(2)}) async-start(), calls=%async_computation.6 | async-start | bytes 2621440 | tf_op jit(solution)/shard_map/all_gather | solution.py:84
  342.3 213.3 %all-reduce.6.cloned.1.call-start = ((), (), s32[]{:S(2)}) async-start(), calls=%async_computation.7 | async-start | bytes 2097152 | tf_op jit(solution)/shard_map/psum | solution.py:16
  426.3 1.7 copy-start.1
  514.7 6.0 copy-start.5
  514.7 6.0 copy-start.6
  520.4 89.0 %all-reduce.8.cloned.1.call-start = ((), (), s32[]{:S(2)}) async-start(), calls=%async_computation.8 | async-start | bytes 2097152 | tf_op jit(solution)/shard_map/psum | solution.py:16
  563.6 9.0 %copy-start.7 = (bf16[2048]{0:T(1024)(128)(2,1)S(1)}, bf16[2048]{0:T(1024)(128)(2,1)}, u32[]{:S(2)}) copy-start(bf16[2048]{0:T(1024)(128)(2,1)} %param.31) | copy-start | bytes 12292
Sparse Core Ops, SparseCore 0:
  8.9 109.3 all-gather.6
  119.9 104.9 all-gather.10
  226.5 104.9 all-gather.8
  340.5 34.5 all-reduce.3
  376.5 46.1 all-gather.14
  424.1 44.4 all-gather.12
  470.2 44.4 all-gather.16
  520.5 35.0 all-reduce.5
  572.6 36.7 all-reduce.7
where the time goes:
time: 621 us; the launch traced here: 620 us
  waiting for transfers between devices  556 us (90%)
  matrix products  36.2 us (6%)
  between operations  13.5 us (2%)
  other arithmetic  12.6 us (2%)
    all_gather x1, waiting for transfers between devices, shards(): lax.all_gather(gate_weight, 'fs', axis=0, tiled=True)  109 us
    all_gather x1, waiting for transfers between devices, shards(): lax.all_gather(up_weight, 'fs', axis=0, tiled=True)  107 us
    psum x3, waiting for transfers between devices, reduce_partial(): return lax.psum(terms.astype(jnp.bfloat16), 'tp').astype(jnp.float32)  104 us
    all_gather x1, waiting for transfers between devices, shards(): down_full = lax.all_gather(down_weight, 'fs', axis=1, tiled=True)  102 us
    all_gather x1, waiting for transfers between devices, shards(): out_full = lax.all_gather(mix_out_weight, 'fs', axis=1, tiled=True)  46.1 us
    all_gather x1, waiting for transfers between devices, shards(): lax.all_gather(mix_v_weight, 'fs', axis=0, tiled=True)  44.1 us
    all_gather x1, waiting for transfers between devices, shards(): lax.all_gather(mix_u_weight, 'fs', axis=0, tiled=True)  40.1 us
    dot_general x2, matrix products, shards(): terms = jnp.dot(hidden, down_full, preferred_element_type=jnp.float32)  17.8 us
  transfers between devices with their start and end apart: 9, of which 9 were waited for; matrix products, arithmetic and copies ran while one was open for 2% of the time, Pallas kernels for 0%

commit v1 on v0

--- a/solution.py
+++ b/solution.py
@@ -69,7 +69,7 @@
         lax.all_gather(gate_weight, "fs", axis=0, tiled=True),
         lax.all_gather(up_weight, "fs", axis=0, tiled=True),
     )
-    down_full = lax.all_gather(down_weight, "fs", axis=1, tiled=True)
+    down_full = jnp.concatenate(lax.all_gather(down_weight, "fs"), axis=1)
     hidden = gated_hidden(normed, gate_full, up_full)
     terms = jnp.dot(hidden, down_full, preferred_element_type=jnp.float32)
     first = add_branch(tokens, terms, ffn_post_gain, 0.5)

time: 621 us -> 621 us (level)
  local copies, waits for them, and re-layouts: 1.03 us -> 9.44 us
  waiting for transfers between devices: 556 us -> 548 us
    all_gather x1, waiting for transfers between devices: 109 us -> 98.1 us  [shards(): lax.all_gather(gate_weight, 'fs', axis=0, tiled=True)]
    reshape x0 -> x1, local copies, waits for them, and re-layouts: none -> 8.42 us  [shards(): down_full = jnp.concatenate(lax.all_gather(down_weight, 'fs'), axis=1)]
    all_gather x1, waiting for transfers between devices: 102 us -> 109 us  [shards(): down_full = jnp.concatenate(lax.all_gather(down_weight, 'fs'), axis=1)]
  transfers between devices with their start and end apart: 9 -> 9, of which waited for: 9 -> 9; matrix products, arithmetic and copies ran while one was open for 2% -> 4% of each run, Pallas kernels for 0% -> 0%
where the time goes in v1:
time: 621 us; the launch traced here: 620 us
  waiting for transfers between devices  548 us (88%)
  matrix products  36 us (6%)
  between operations  13.5 us (2%)
  other arithmetic  12.5 us (2%)
  local copies, waits for them, and re-layouts  9.44 us (2%)
    all_gather x1, waiting for transfers between devices, shards(): down_full = jnp.concatenate(lax.all_gather(down_weight, 'fs'), axis=1)  109 us
    psum x3, waiting for transfers between devices, reduce_partial(): return lax.psum(terms.astype(jnp.bfloat16), 'tp').astype(jnp.float32)  104 us
    all_gather x1, waiting for transfers between devices, shards(): lax.all_gather(up_weight, 'fs', axis=0, tiled=True)  102 us
    all_gather x1, waiting for transfers between devices, shards(): lax.all_gather(gate_weight, 'fs', axis=0, tiled=True)  98.1 us
    all_gather x1, waiting for transfers between devices, shards(): out_full = lax.all_gather(mix_out_weight, 'fs', axis=1, tiled=True)  46.1 us
    all_gather x1, waiting for transfers between devices, shards(): lax.all_gather(mix_v_weight, 'fs', axis=0, tiled=True)  44.1 us
    all_gather x1, waiting for transfers between devices, shards(): lax.all_gather(mix_u_weight, 'fs', axis=0, tiled=True)  40.2 us
    dot_general x2, matrix products, shards(): terms = jnp.dot(hidden, down_full, preferred_element_type=jnp.float32)  17.7 us
  transfers between devices with their start and end apart: 9, of which 9 were waited for; matrix products, arithmetic and copies ran while one was open for 4% of the time, Pallas kernels for 0%

profile of v1, /device:TPU:0, one launch (start us, length us, event | category | flops | bytes accessed | tf_op | source)
XLA Modules:
  0.0 620.1 jit_solution(16838903782644297452)
XLA Ops:
  6.5 0.7 all-gather.18.cloned.1.call-update
  9.1 109.2 %all-gather.18.cloned.1.call-done = bf16[5632,512]{1,0:T(8,128)(2,1)} async-done(((bf16[1408,512]{1,0:T(8,128)(2,1)}), bf16[5632,512]{1,0:T(8,128)(2,1)}) %all-gather.18.cloned.1.call-update) | async-done | bytes 5767184 | tf_op jit(solution)/shard_map/all_gather | solution.py:72
  118.3 8.4 %copy.34 = bf16[1408,4,512]{0,2,1:T(8,128)(2,1)} copy(bf16[1408,4,512]{2,0,1:T(8,128)(2,1)} %bitcast.39) | data formatting | bytes 11534336 | tf_op jit(solution)/shard_map/reshape | solution.py:72
  126.8 98.1 %all-gather.8.cloned.1.call-done = bf16[2048,1408]{1,0:T(8,128)(2,1)} async-done(((bf16[512,1408]{1,0:T(8,128)(2,1)}), bf16[2048,1408]{1,0:T(8,128)(2,1)}) %all-gather.8.cloned.1.call-update) | async-done | bytes 5767184 | tf_op jit(solution)/shard_map/all_gather | solution.py:69
  224.9 4.5 fusion.59
  229.4 102.1 %all-gather.10.cloned.1.call-done = bf16[2048,1408]{1,0:T(8,128)(2,1)} async-done(((bf16[512,1408]{1,0:T(8,128)(2,1)}), bf16[2048,1408]{1,0:T(8,128)(2,1)}) %all-gather.10.cloned.1.call-update) | async-done | bytes 5767184 | tf_op jit(solution)/shard_map/all_gather | solution.py:70
  331.4 8.9 %convolution_convert_fusion.2 = bf16[256,2048]{1,0:T(8,128)(2,1)} fusion(bf16[1408,2048]{0,1:T(8,128)(2,1)} %bitcast.37, bf16[2048,1408]{1,0:T(8,128)(2,1)} %all-gather.10.cloned.1.call-done, f32[256,1408]{1,0:T(8,128)S(1)} %fusion.59, bf16[256,2048]{1,0:T(8,128)(2,1)S(1)} %copy-done, f32[2048]{0:T(1024)S(1)} %convert_element_type.82, ...), kind=kOutput, calls=%fused_computation.21 | convolution fusion | flops 2957574144 | bytes 15082496 | tf_op jit(solution)/shard_map/dot_general | solution.py:74
  341.6 0.7 all-gather.16.cloned.1.call-update
  342.6 32.5 %all-reduce.4.cloned.1.call-done = bf16[256,2048]{1,0:T(8,128)(2,1)} async-done(((bf16[256,2048]{1,0:T(8,128)(2,1)}), bf16[256,2048]{1,0:T(8,128)(2,1)}) %all-reduce.4.cloned.1.call-update) | async-done | bytes 1048592 | tf_op jit(solution)/shard_map/psum | solution.py:16
  375.1 1.5 fusion.2
  376.6 2.0 fusion.14
  378.5 44.1 %all-gather.14.cloned.1.call-done = bf16[2048,512]{1,0:T(8,128)(2,1)} async-done(((bf16[512,512]{1,0:T(8,128)(2,1)}), bf16[2048,512]{1,0:T(8,128)(2,1)}) %all-gather.14.cloned.1.call-update) | async-done | bytes 2097168 | tf_op jit(solution)/shard_map/all_gather | solution.py:79
  422.6 3.4 fusion.28
  428.4 40.2 %all-gather.12.cloned.1.call-done = bf16[2048,512]{1,0:T(8,128)(2,1)} async-done(((bf16[512,512]{1,0:T(8,128)(2,1)}), bf16[2048,512]{1,0:T(8,128)(2,1)}) %all-gather.12.cloned.1.call-update) | async-done | bytes 2097168 | tf_op jit(solution)/shard_map/all_gather | solution.py:78
  468.6 46.1 %all-gather.16.cloned.1.call-done = bf16[512,2048]{1,0:T(8,128)(2,1)} async-done(((bf16[512,512]{1,0:T(8,128)(2,1)}), bf16[512,2048]{1,0:T(8,128)(2,1)}) %all-gather.16.cloned.1.call-update) | async-done | bytes 2097168 | tf_op jit(solution)/shard_map/all_gather | solution.py:84
  514.6 5.7 convolution_convert_fusion
  520.7 34.9 %all-reduce.6.cloned.1.call-done = bf16[256,2048]{1,0:T(8,128)(2,1)} async-done(((bf16[256,2048]{1,0:T(8,128)(2,1)}), bf16[256,2048]{1,0:T(8,128)(2,1)}) %all-reduce.6.cloned.1.call-update) | async-done | bytes 1048592 | tf_op jit(solution)/shard_map/psum | solution.py:16
  555.6 1.5 fusion.5
  557.1 1.9 fusion.18
  559.0 4.5 fusion.45
  563.5 8.8 %convolution_convert_fusion.1 = bf16[256,2048]{1,0:T(8,128)(2,1)} fusion(bf16[1408,2048]{0,1:T(8,128)(2,1)} %bitcast.38, bf16[2048,1408]{1,0:T(8,128)(2,1)} %all-gather.10.cloned.1.call-done, f32[256,1408]{1,0:T(8,128)S(1)} %fusion.45, bf16[256,2048]{1,0:T(8,128)(2,1)S(1)} %get-tuple-element.6, f32[2048]{0:T(1024)S(1)} %convert_element_type.99, ...), kind=kOutput, calls=%fused_computation.20 | convolution fusion | flops 2957574144 | bytes 15082496 | tf_op jit(solution)/shard_map/dot_general | solution.py:89
  572.4 36.9 %all-reduce.8.cloned.1.call-done = bf16[256,2048]{1,0:T(8,128)(2,1)} async-done(((bf16[256,2048]{1,0:T(8,128)(2,1)}), bf16[256,2048]{1,0:T(8,128)(2,1)}) %all-reduce.8.cloned.1.call-update) | async-done | bytes 1048592 | tf_op jit(solution)/shard_map/psum | solution.py:16
  609.3 1.5 fusion.7
  610.8 2.8 fusion.21
  (63 shorter events, 5.9 us)
Async XLA Ops:
  6.5 2.3 copy-start.2
  6.5 2.3 copy-start
  6.5 111.8 %all-gather.18.cloned.1.call-start = ((), (), s32[]{:S(2)}) async-start(), calls=%async_computation.8 | async-start | bytes 7208960 | tf_op jit(solution)/shard_map/all_gather | solution.py:72
  7.3 217.6 %all-gather.8.cloned.1.call-start = ((), (), s32[]{:S(2)}) async-start(), calls=%async_computation | async-start | bytes 7208960 | tf_op jit(solution)/shard_map/all_gather | solution.py:69
  8.0 323.4 %all-gather.10.cloned.1.call-start = ((), (), s32[]{:S(2)}) async-start(), calls=%async_computation.1 | async-start | bytes 7208960 | tf_op jit(solution)/shard_map/all_gather | solution.py:70
  8.7 366.3 %all-reduce.4.cloned.1.call-start = ((), (), s32[]{:S(2)}) async-start(), calls=%async_computation.2 | async-start | bytes 2097152 | tf_op jit(solution)/shard_map/psum | solution.py:16
  340.3 2.2 copy-start.3
  340.3 2.2 copy-start.4
  340.3 2.2 copy-start.8
  340.3 2.3 copy-start.9
  340.4 82.3 %all-gather.14.cloned.1.call-start = ((), (), s32[]{:S(2)}) async-start(), calls=%async_computation.4 | async-start | bytes 2621440 | tf_op jit(solution)/shard_map/all_gather | solution.py:79
  340.9 127.6 %all-gather.12.cloned.1.call-start = ((), (), s32[]{:S(2)}) async-start(), calls=%async_computation.3 | async-start | bytes 2621440 | tf_op jit(solution)/shard_map/all_gather | solution.py:78
  341.5 173.1 %all-gather.16.cloned.1.call-start = ((), (), s32[]{:S(2)}) async-start(), calls=%async_computation.5 | async-start | bytes 2621440 | tf_op jit(solution)/shard_map/all_gather | solution.py:84
  342.3 213.3 %all-reduce.6.cloned.1.call-start = ((), (), s32[]{:S(2)}) async-start(), calls=%async_computation.6 | async-start | bytes 2097152 | tf_op jit(solution)/shard_map/psum | solution.py:16
  426.2 1.6 copy-start.1
  514.6 6.0 copy-start.5
  514.6 6.0 copy-start.6
  520.4 88.9 %all-reduce.8.cloned.1.call-start = ((), (), s32[]{:S(2)}) async-start(), calls=%async_computation.7 | async-start | bytes 2097152 | tf_op jit(solution)/shard_map/psum | solution.py:16
  563.5 8.8 %copy-start.7 = (bf16[2048]{0:T(1024)(128)(2,1)S(1)}, bf16[2048]{0:T(1024)(128)(2,1)}, u32[]{:S(2)}) copy-start(bf16[2048]{0:T(1024)(128)(2,1)} %param.31) | copy-start | bytes 12292
Sparse Core Ops, SparseCore 0:
  8.9 109.3 all-gather.17
  119.9 104.9 all-gather.7
  226.5 104.9 all-gather.9
  340.5 34.5 all-reduce.3
  376.5 46.1 all-gather.13
  424.1 44.4 all-gather.11
  470.1 44.4 all-gather.15
  520.5 35.0 all-reduce.5
  572.5 36.7 all-reduce.7
